TPU v7x, 32 devices: a whole 2x2x4 slice. The times are simulated.
32 devices in a mesh: rep: 2 (over y), fs: 4 (over z), tp: 4 (over x, core).
Axes of the slice: x: 2, y: 2, z: 4, core: 2. Of those that a mesh axis runs over, the one named last changes fastest.
Arguments:
- stream: bfloat16 [2048, 1536], P(('rep', 'fs')), may hold values from -6 to 6
- mix_pre_gain: float32 [1536], replicated, may hold values from 0.1 to 1.9
- w_outer_gate: bfloat16 [1536, 768], P('fs', 'tp'), may hold values from -0.15625 to 0.15625
- w_inner_gate: bfloat16 [1536, 768], P('fs', 'tp'), may hold values from -0.15625 to 0.15625
- w_value: bfloat16 [1536, 768], P('fs', 'tp'), may hold values from -0.15625 to 0.15625
- mix_taps: float32 [3, 768], P(None, 'tp'), may hold values from -3 to 3
- w_mix_out: bfloat16 [768, 1536], P('tp', 'fs'), may hold values from -0.3125 to 0.3125
- mix_post_gain: float32 [1536], replicated, may hold values from 0.1 to 1.9
- ffn_pre_gain: float32 [1536], replicated, may hold values from 0.1 to 1.9
- w_linear: bfloat16 [1536, 4224], P('fs', 'tp'), may hold values from -0.15625 to 0.15625
- w_gated: bfloat16 [1536, 4224], P('fs', 'tp'), may hold values from -0.15625 to 0.15625
- ffn_taps: float32 [3, 4224], P(None, 'tp'), may hold values from -3 to 3
- ffn_bias: float32 [4224], P('tp'), may hold values from -3 to 3
- w_down: bfloat16 [4224, 1536], P('tp', 'fs'), may hold values from -0.125 to 0.125
- ffn_post_gain: float32 [1536], replicated, may hold values from 0.1 to 1.9
Outputs:
- result: bfloat16 [2048, 1536], P(('rep', 'fs'))
All inputs are finite; a program needn't handle non-finite values.
Results may differ from a plain program's by a relative error of at most 0.023.
Values may be sent and summed in bfloat16 or wider, within the bound.
A program may use at most 64 MiB of HBM per device.

v0:
```python
import jax
import jax.numpy as jnp
from jax import lax
from jax.sharding import PartitionSpec as P

SEQ_LEN = 128


EPS = 1e-06


def norm_scale(values, gain):
    return values * lax.rsqrt(jnp.mean(values * values, axis=-1, keepdims=True) + EPS) * gain


def conv_three(values, taps):
    height, breadth = values.shape
    grouped = values.reshape(height // SEQ_LEN, SEQ_LEN, breadth)
    padded = jnp.pad(grouped, ((0, 0), (1, 1), (0, 0)))
    mixed = taps[0] * padded[:, :-2] + taps[1] * padded[:, 1:-1] + taps[2] * padded[:, 2:]
    return mixed.reshape(height, breadth)


def settle(partial_value, resid, post_gain):
    branch = lax.psum(partial_value.astype(jnp.bfloat16), "tp")
    return (resid + norm_scale(branch.astype(jnp.float32), post_gain)).astype(jnp.bfloat16)


def on_device(
    stream,
    mix_pre_gain,
    w_outer_gate,
    w_inner_gate,
    w_value,
    mix_taps,
    w_mix_out,
    mix_post_gain,
    ffn_pre_gain,
    w_linear,
    w_gated,
    ffn_taps,
    ffn_bias,
    w_down,
    ffn_post_gain,
):
    resid = stream.astype(jnp.float32)
    normed = norm_scale(resid, mix_pre_gain).astype(jnp.bfloat16)
    full_outer, full_inner, full_value = (
        lax.all_gather(w_outer_gate, "fs", axis=0, tiled=True),
        lax.all_gather(w_inner_gate, "fs", axis=0, tiled=True),
        lax.all_gather(w_value, "fs", axis=0, tiled=True),
    )
    outer = jnp.dot(normed, full_outer, preferred_element_type=jnp.float32)
    inner = jnp.dot(normed, full_inner, preferred_element_type=jnp.float32)
    value = jnp.dot(normed, full_value, preferred_element_type=jnp.float32)
    outer = outer.astype(jnp.bfloat16)
    inner = inner.astype(jnp.bfloat16)
    value = value.astype(jnp.bfloat16)
    product = inner.astype(jnp.float32) * value.astype(jnp.float32)
    mixed = (outer.astype(jnp.float32) * conv_three(product, mix_taps)).astype(jnp.bfloat16)
    full_mix_out = lax.all_gather(w_mix_out, "fs", axis=1, tiled=True)
    partial_value = jnp.dot(mixed, full_mix_out, preferred_element_type=jnp.float32)
    middle = settle(partial_value, resid, mix_post_gain)
    middle_f = middle.astype(jnp.float32)
    normed_two = norm_scale(middle_f, ffn_pre_gain).astype(jnp.bfloat16)
    full_linear, full_gated = (
        lax.all_gather(w_linear, "fs", axis=0, tiled=True),
        lax.all_gather(w_gated, "fs", axis=0, tiled=True),
    )
    linear = jnp.dot(normed_two, full_linear, preferred_element_type=jnp.float32)
    gated = jnp.dot(normed_two, full_gated, preferred_element_type=jnp.float32)
    linear = linear.astype(jnp.bfloat16)
    gated = gated.astype(jnp.bfloat16)
    activated = jax.nn.gelu(
        conv_three(gated.astype(jnp.float32), ffn_taps) + ffn_bias, approximate=True
    )
    hidden = (activated * linear.astype(jnp.float32)).astype(jnp.bfloat16)
    full_down = lax.all_gather(w_down, "fs", axis=1, tiled=True)
    partial_two = jnp.dot(hidden, full_down, preferred_element_type=jnp.float32)
    return settle(partial_two, middle_f, ffn_post_gain)


def solution(mesh):
    in_specs = (
        P(("rep", "fs"), None),
        P(),
        P("fs", "tp"),
        P("fs", "tp"),
        P("fs", "tp"),
        P(None, "tp"),
        P("tp", "fs"),
        P(),
        P(),
        P("fs", "tp"),
        P("fs", "tp"),
        P(None, "tp"),
        P("tp"),
        P("tp", "fs"),
        P(),
    )
    out_specs = P(("rep", "fs"), None)
    return jax.shard_map(
        on_device, mesh=mesh, in_specs=in_specs, out_specs=out_specs, check_vma=False
    )
```

profile of v0, /device:TPU:1, one launch (start us, length us, event | category | flops | bytes accessed | tf_op | source)
XLA Modules:
  0.0 329.2 jit_solution(645357725762932306)
XLA Ops:
  7.4 0.0 all-reduce.5.cloned.1.call-start
  7.4 1.5 fusion.8
  8.8 16.0 %all_gather.22 = bf16[1536,192]{0,1:T(8,128)(2,1)S(1)} all-gather(bf16[384,192]{0,1:T(8,128)(2,1)} %param.18), channel_id=1, replica_groups=mesh['rep'=2,'fs'=4,'tp'=4] {'fs'}, dimensions={0}, use_global_device_ids=true | all-gather | bytes 737280 | tf_op jit(solution)/shard_map/all_gather | solution.py:50
  24.8 0.0 copy-done.1
  24.8 12.2 %all_gather.23 = bf16[1536,192]{0,1:T(8,128)(2,1)S(1)} all-gather(bf16[384,192]{0,1:T(8,128)(2,1)S(1)} %copy-done.1), channel_id=1, replica_groups=mesh['rep'=2,'fs'=4,'tp'=4] {'fs'}, dimensions={0}, use_global_device_ids=true | all-gather | bytes 737280 | tf_op jit(solution)/shard_map/all_gather | solution.py:51
  37.0 0.0 copy-done
  37.0 0.0 copy-done.8
  37.1 0.5 fusion.18
  37.6 0.0 copy-start.7
  37.6 0.0 copy-start.2
  37.6 0.0 copy-start.3
  37.6 0.5 fusion.17
  38.1 0.1 reshape.58
  38.2 0.0 copy-done.7
  38.3 0.2 copy-done.2
  38.5 13.3 %all_gather.21 = bf16[1536,192]{0,1:T(8,128)(2,1)S(1)} all-gather(bf16[384,192]{0,1:T(8,128)(2,1)S(1)} %copy-done.2), channel_id=1, replica_groups=mesh['rep'=2,'fs'=4,'tp'=4] {'fs'}, dimensions={0}, use_global_device_ids=true | all-gather | bytes 737280 | tf_op jit(solution)/shard_map/all_gather | solution.py:49
  51.8 0.0 copy-done.3
  51.8 14.4 %all_gather.24 = bf16[192,1536]{1,0:T(8,128)(2,1)S(1)} all-gather(bf16[192,384]{1,0:T(8,128)(2,1)S(1)} %copy-done.3), channel_id=1, replica_groups=mesh['rep'=2,'fs'=4,'tp'=4] {'fs'}, dimensions={1}, use_global_device_ids=true | all-gather | bytes 737280 | tf_op jit(solution)/shard_map/all_gather | solution.py:61
  66.2 1.2 fusion.43
  67.4 2.1 convolution_convert_fusion.3
  69.5 0.0 all-reduce.5.cloned.1.call-update
  69.6 0.0 copy-start.5
  69.6 0.0 all-gather.4.cloned.1.call-start
  69.6 0.5 all-gather.4.cloned.1.call-update
  70.2 0.0 all-gather.6.cloned.1.call-start
  70.2 0.5 all-gather.6.cloned.1.call-update
  70.8 0.0 all-gather.8.cloned.1.call-start
  70.8 0.5 all-gather.8.cloned.1.call-update
  71.3 0.0 all-reduce.7.cloned.1.call-start
  71.4 0.0 copy-done.4
  71.4 0.0 copy-start.9
  71.5 43.6 %all-reduce.5.cloned.1.call-done = bf16[256,1536]{1,0:T(8,128)(2,1)} async-done(((bf16[256,1536]{1,0:T(8,128)(2,1)}), bf16[256,1536]{1,0:T(8,128)(2,1)}) %all-reduce.5.cloned.1.call-update) | async-done | bytes 786448 | tf_op jit(solution)/shard_map/psum | solution.py:25
  115.0 1.4 fusion.4
  116.4 0.0 copy-done.5
  116.4 1.7 fusion.12
  118.1 29.8 %all-gather.4.cloned.1.call-done = bf16[1536,1056]{0,1:T(8,128)(2,1)} async-done(((bf16[384,1056]{0,1:T(8,128)(2,1)}), bf16[1536,1056]{0,1:T(8,128)(2,1)}) %all-gather.4.cloned.1.call-update) | async-done | bytes 3244048 | tf_op jit(solution)/shard_map/all_gather | solution.py:68
  147.9 0.0 copy-done.9
  147.9 4.0 %fusion.2 = f32[256,1056]{0,1:T(8,128)} fusion(bf16[1536,1056]{0,1:T(8,128)(2,1)} %all-gather.4.cloned.1.call-done, bf16[256,1536]{1,0:T(8,128)(2,1)S(1)} %get-tuple-element.9, f32[1536]{0:T(1024)S(1)} %copy-done.9, f32[256]{0:T(256)S(1)} %add_rsqrt_fusion.1), kind=kOutput, calls=%fused_computation.4 | convolution fusion | flops 832585728 | bytes 5118976 | tf_op jit(solution)/shard_map/dot_general | solution.py:71
  151.9 1.8 reshape.64
  153.7 0.0 copy-start.10
  153.7 7.3 %fusion.31 = f32[2,128,1056]{1,0,2:T(2,128)} fusion(f32[2,128,1056]{1,0,2:T(2,128)S(1)} %reshape.64, f32[1056]{0:T(1024)S(1)} %get-tuple-element.6, f32[1056]{0:T(1024)S(1)} %get-tuple-element.7, f32[1056]{0:T(1024)S(1)} %get-tuple-element.5), kind=kLoop, calls=%fused_computation.51 | loop fusion | flops 1351680 | bytes 2175360 | tf_op jit(solution)/shard_map/add | solution.py:20
  161.1 51.6 %all-gather.6.cloned.1.call-done = bf16[1536,1056]{0,1:T(8,128)(2,1)} async-done(((bf16[384,1056]{0,1:T(8,128)(2,1)}), bf16[1536,1056]{0,1:T(8,128)(2,1)}) %all-gather.6.cloned.1.call-update) | async-done | bytes 3244048 | tf_op jit(solution)/shard_map/all_gather | solution.py:67
  212.7 64.8 %all-gather.8.cloned.1.call-done = bf16[1056,1536]{1,0:T(8,128)(2,1)} async-done(((bf16[1056,384]{1,0:T(8,128)(2,1)}), bf16[1056,1536]{1,0:T(8,128)(2,1)}) %all-gather.8.cloned.1.call-update) | async-done | bytes 3244048 | tf_op jit(solution)/shard_map/all_gather | solution.py:78
  277.4 7.9 %convolution_convert_fusion.2 = bf16[256,1536]{1,0:T(8,128)(2,1)} fusion(bf16[1056,1536]{1,0:T(8,128)(2,1)} %all-gather.8.cloned.1.call-done, bf16[1536,1056]{0,1:T(8,128)(2,1)} %all-gather.6.cloned.1.call-done, f32[132,8,2,128]{3,2,1,0:T(2,128)} %bitcast.31, f32[1056]{0:T(1024)S(1)} %copy-done.10, bf16[256,1536]{1,0:T(8,128)(2,1)S(1)} %get-tuple-element.9, ...), kind=kOutput, calls=%fused_computation.6 | convolution fusion | flops 1666424832 | bytes 9153664 | tf_op jit(solution)/shard_map/dot_general | solution.py:79
  285.4 0.0 all-reduce.7.cloned.1.call-update
  285.4 32.5 %all-reduce.7.cloned.1.call-done = bf16[256,1536]{1,0:T(8,128)(2,1)} async-done(((bf16[256,1536]{1,0:T(8,128)(2,1)}), bf16[256,1536]{1,0:T(8,128)(2,1)}) %all-reduce.7.cloned.1.call-update) | async-done | bytes 786448 | tf_op jit(solution)/shard_map/psum | solution.py:25
  317.9 1.4 fusion.6
  319.3 2.4 fusion.15
  (13 shorter events, 0.1 us)
Async XLA Ops:
  7.4 29.7 %copy-start = (bf16[256,1536]{1,0:T(8,128)(2,1)S(1)}, bf16[256,1536]{1,0:T(8,128)(2,1)}, u32[]{:S(2)}) copy-start(bf16[256,1536]{1,0:T(8,128)(2,1)} %param.15) | copy-start | bytes 2359300
  7.4 17.4 %copy-start.1 = (bf16[384,192]{0,1:T(8,128)(2,1)S(1)}, bf16[384,192]{0,1:T(8,128)(2,1)}, u32[]{:S(2)}) copy-start(bf16[384,192]{0,1:T(8,128)(2,1)} %param.19) | copy-start | bytes 442372
  7.4 29.7 %copy-start.8 = (f32[1536]{0:T(1024)S(1)}, f32[1536]{0:T(1024)}, u32[]{:S(2)}) copy-start(f32[1536]{0:T(1024)} %param.16) | copy-start | bytes 18436
  7.4 107.7 %all-reduce.5.cloned.1.call-start = ((), (), s32[]{:S(2)}) async-start(), calls=%async_computation | async-start | bytes 1572864 | tf_op jit(solution)/shard_map/psum | solution.py:25
  37.6 0.7 copy-start.7
  37.6 0.9 copy-start.2
  37.6 14.2 %copy-start.3 = (bf16[192,384]{1,0:T(8,128)(2,1)S(1)}, bf16[192,384]{1,0:T(8,128)(2,1)}, u32[]{:S(2)}) copy-start(bf16[192,384]{1,0:T(8,128)(2,1)} %param.21) | copy-start | bytes 442372
  69.5 1.8 copy-start.4
  69.6 46.8 %copy-start.5 = (f32[1536]{0:T(1024)S(1)}, f32[1536]{0:T(1024)}, u32[]{:S(2)}) copy-start(f32[1536]{0:T(1024)} %param.22) | copy-start | bytes 18436
  69.6 78.3 %all-gather.4.cloned.1.call-start = ((), (), s32[]{:S(2)}) async-start(), calls=%async_computation.1 | async-start | bytes 4055040 | tf_op jit(solution)/shard_map/all_gather | solution.py:68
  70.2 142.5 %all-gather.6.cloned.1.call-start = ((), (), s32[]{:S(2)}) async-start(), calls=%async_computation.2 | async-start | bytes 4055040 | tf_op jit(solution)/shard_map/all_gather | solution.py:67
  70.8 206.7 %all-gather.8.cloned.1.call-start = ((), (), s32[]{:S(2)}) async-start(), calls=%async_computation.3 | async-start | bytes 4055040 | tf_op jit(solution)/shard_map/all_gather | solution.py:78
  71.3 246.6 %all-reduce.7.cloned.1.call-start = ((), (), s32[]{:S(2)}) async-start(), calls=%async_computation.4 | async-start | bytes 1572864 | tf_op jit(solution)/shard_map/psum | solution.py:25
  71.4 76.4 %copy-start.9 = (f32[1536]{0:T(1024)S(1)}, f32[1536]{0:T(1024)}, u32[]{:S(2)}) copy-start(f32[1536]{0:T(1024)} %param.23) | copy-start | bytes 18436
  153.7 123.7 %copy-start.10 = (f32[1056]{0:T(1024)S(1)}, f32[1056]{0:T(1024)}, u32[]{:S(2)}) copy-start(f32[1056]{0:T(1024)} %param.27) | copy-start | bytes 12676
  285.4 33.9 %copy-start.6 = (f32[1536]{0:T(1024)S(1)}, f32[1536]{0:T(1024)}, u32[]{:S(2)}) copy-start(f32[1536]{0:T(1024)} %param.29) | copy-start | bytes 18436
Sparse Core Ops, SparseCore 0:
  69.7 45.2 all-reduce.4
  285.5 32.3 all-reduce.6
Sparse Core Ops, SparseCore 1:
  71.7 76.1 all-gather.3
  149.3 63.3 all-gather.5
  214.1 63.3 all-gather.7
where the time goes:
time: 332 us; the launch traced here: 329 us
  waiting for transfers between devices  224 us (67%)
  blocking collectives  56 us (17%)
  other arithmetic  16.8 us (5%)
  between operations  15.2 us (5%)
  matrix products  15.1 us (5%)
    psum x2, waiting for transfers between devices, settle(): branch = lax.psum(partial_value.astype(jnp.bfloat16), 'tp')  76.1 us
    all_gather x1, waiting for transfers between devices, on_device(): full_down = lax.all_gather(w_down, 'fs', axis=1, tiled=True)  64.8 us
    all_gather x1, waiting for transfers between devices, on_device(): lax.all_gather(w_linear, 'fs', axis=0, tiled=True)  51.6 us
    all_gather x1, waiting for transfers between devices, on_device(): lax.all_gather(w_gated, 'fs', axis=0, tiled=True)  29.8 us
    all_gather x1, blocking collectives, on_device(): lax.all_gather(w_inner_gate, 'fs', axis=0, tiled=True)  16 us
    all_gather x1, blocking collectives, on_device(): full_mix_out = lax.all_gather(w_mix_out, 'fs', axis=1, tiled=True)  14.4 us
    all_gather x1, blocking collectives, on_device(): lax.all_gather(w_outer_gate, 'fs', axis=0, tiled=True)  13.3 us
    all_gather x1, blocking collectives, on_device(): lax.all_gather(w_value, 'fs', axis=0, tiled=True)  12.2 us
  transfers between devices with their start and end apart: 5, of which 5 were waited for; matrix products, arithmetic and copies ran while one was open for 5% of the time, Pallas kernels for 0%

commit v1 on v0

--- a/solution.py
+++ b/solution.py
@@ -1,9 +1,14 @@
+import functools
+
 import jax
 import jax.numpy as jnp
 from jax import lax
+from jax.experimental import pallas as pl
+from jax.experimental.pallas import tpu as pltpu
 from jax.sharding import PartitionSpec as P
 
 SEQ_LEN = 128
+PACK = 16
 
 
 EPS = 1e-06
@@ -26,7 +31,7 @@
     return (resid + norm_scale(branch.astype(jnp.float32), post_gain)).astype(jnp.bfloat16)
 
 
-def on_device(
+def gather_plan(
     stream,
     mix_pre_gain,
     w_outer_gate,
@@ -80,6 +85,381 @@
     return settle(partial_two, middle_f, ffn_post_gain)
 
 
+ORDER = (1, 3, 2)
+
+
+def dot_nt(left, right):
+    return lax.dot_general(left, right, (((1,), (1,)), ((), ())), preferred_element_type=jnp.float32)
+
+
+def dot_nn(left, right):
+    return jnp.dot(left, right, preferred_element_type=jnp.float32)
+
+
+def conv_rows(values, taps):
+    height = values.shape[0]
+    row = lax.broadcasted_iota(jnp.int32, values.shape, 0) % SEQ_LEN
+    before = jnp.where(row == 0, 0.0, pltpu.roll(values, 1, 0))
+    after = jnp.where(row == SEQ_LEN - 1, 0.0, pltpu.roll(values, height - 1, 0))
+    return taps[0:1] * before + taps[1:2] * values + taps[2:3] * after
+
+
+def kernel(
+    n_fs,
+    conv_w,
+    hid,
+    stream,
+    gains,
+    mix_w,
+    mix_taps,
+    ffn_w,
+    ffn_small,
+    out,
+    mix_all,
+    ffn_all,
+    xs,
+    normed,
+    middle,
+    pm,
+    rm,
+    sm,
+    rxm,
+    bm,
+    pf,
+    rf,
+    sf,
+    rxf,
+    tf,
+    rz,
+    bf,
+    zs_s,
+    zs_r,
+    mix_s,
+    mix_r,
+    ag_s,
+    ag_r,
+    rs_s,
+    rs_r,
+    fin_s,
+    fin_r,
+):
+    r, f, t = lax.axis_index("rep"), lax.axis_index("fs"), lax.axis_index("tp")
+    x, c = t // 2, t % 2
+    core = {"tp": 2 * x + 1 - c}
+    side = {"tp": 2 * (1 - x) + c}
+    t_side = 2 * (1 - x) + c
+    other = {"rep": 1 - r}
+    rows, width = stream.shape[0], mix_w.shape[1]
+    n_seq = rows // SEQ_LEN
+    mix_half, ffn_half = mix_w.shape[0] // 2, ffn_w.shape[1] // 2
+
+    def send(src, dst, ss, rs, where):
+        return pltpu.make_async_remote_copy(
+            src_ref=src,
+            dst_ref=dst,
+            send_sem=ss,
+            recv_sem=rs,
+            device_id=where,
+            device_id_type=pl.DeviceIdType.MESH,
+        )
+
+    barrier = pltpu.get_barrier_semaphore()
+    peers = [core, side, other] + [{"fs": (f + k) % n_fs} for k in ORDER]
+    for peer in peers:
+        pl.semaphore_signal(barrier, inc=1, device_id=peer, device_id_type=pl.DeviceIdType.MESH)
+    pl.semaphore_wait(barrier, len(peers))
+
+    mix_rows = pl.ds(pl.multiple_of(r * mix_half, PACK), mix_half)
+    ffn_rows = pl.ds(pl.multiple_of(r * ffn_half, PACK), ffn_half)
+    mix_z, ffn_z = {}, {}
+    for k in ORDER:
+        to = {"fs": (f + k) % n_fs}
+        mix_z[k] = send(mix_w.at[mix_rows], mix_all.at[f, mix_rows], zs_s.at[0, k], zs_r.at[0, k], to)
+        mix_z[k].start()
+    for k in ORDER:
+        to = {"fs": (f + k) % n_fs}
+        ffn_z[k] = send(
+            ffn_w.at[(f + k) % n_fs, ffn_rows], ffn_all.at[f, ffn_rows], zs_s.at[1, k], zs_r.at[1, k], to
+        )
+        ffn_z[k].start()
+
+    mix_all[f] = mix_w[...]
+    ffn_all[f] = ffn_w[f]
+
+    def norm_rows(values, gain):
+        scale = lax.rsqrt(jnp.mean(values * values, axis=-1, keepdims=True) + EPS)
+        return values * scale * gain
+
+    step_rows = 32
+
+    @pl.loop(0, rows // step_rows)
+    def _(i):
+        at = pl.ds(pl.multiple_of(i * step_rows, step_rows), step_rows)
+        normed[at] = norm_rows(stream[at].astype(jnp.float32), gains[0:1]).astype(jnp.bfloat16)
+
+    mix_y = {}
+    for k in ORDER:
+        mix_z[k].wait_recv()
+        src = mix_all.at[(f - k + n_fs) % n_fs, mix_rows]
+        mix_y[k] = send(src, src, zs_s.at[2, k], zs_r.at[2, k], other)
+        mix_y[k].start()
+    for k in ORDER:
+        mix_y[k].wait_recv()
+
+    mix_core, mix_side, mix_back = {}, {}, {}
+    for q in range(n_seq):
+        here = slice(q * SEQ_LEN, (q + 1) * SEQ_LEN)
+        parts = []
+        for p in range(3):
+            total = 0.0
+            for j in range(n_fs):
+                total = total + dot_nt(
+                    normed[here, j * width : (j + 1) * width], mix_all[j, p * conv_w : (p + 1) * conv_w]
+                )
+            parts.append(total.astype(jnp.bfloat16).astype(jnp.float32))
+        mixed = (parts[0] * conv_rows(parts[1] * parts[2], mix_taps)).astype(jnp.bfloat16)
+        for j in range(n_fs):
+            pm[q, j % 2, j // 2] = dot_nn(mixed, mix_all[j, 3 * conv_w : 4 * conv_w]).astype(jnp.bfloat16)
+        mix_core[q] = send(pm.at[q, 1 - c], rm.at[q], mix_s.at[0, q], mix_r.at[0, q], core)
+        mix_core[q].start()
+    for q in range(n_seq):
+        mix_core[q].wait_recv()
+        sm[q] = (pm[q, c].astype(jnp.float32) + rm[q].astype(jnp.float32)).astype(jnp.bfloat16)
+        mix_side[q] = send(sm.at[q], rxm.at[q], mix_s.at[1, q], mix_r.at[1, q], side)
+        mix_side[q].start()
+    ffn_y = {}
+
+    def forward(k):
+        ffn_z[k].wait_recv()
+        src = ffn_all.at[(f - k + n_fs) % n_fs, ffn_rows]
+        ffn_y[k] = send(src, src, zs_s.at[3, k], zs_r.at[3, k], other)
+        ffn_y[k].start()
+
+    for q in range(n_seq):
+        mix_side[q].wait_recv()
+        bm[q, c] = (sm[q].astype(jnp.float32) + rxm[q].astype(jnp.float32)).astype(jnp.bfloat16)
+        mix_back[q] = send(bm.at[q, c], bm.at[q, c], mix_s.at[2, q], mix_r.at[2, q], core)
+        mix_back[q].start()
+    for q in range(n_seq):
+        mix_back[q].wait_recv()
+
+        @pl.loop(0, SEQ_LEN // step_rows)
+        def _(i):
+            at = pl.ds(pl.multiple_of(i * step_rows, step_rows), step_rows)
+            to = pl.ds(pl.multiple_of(q * SEQ_LEN + i * step_rows, step_rows), step_rows)
+            branch = jnp.concatenate([bm[q, j % 2, j // 2, at] for j in range(n_fs)], axis=1)
+            mid = stream[to].astype(jnp.float32) + norm_rows(branch.astype(jnp.float32), gains[1:2])
+            mid = mid.astype(jnp.bfloat16)
+            middle[to] = mid
+            two = norm_rows(mid.astype(jnp.float32), gains[2:3]).astype(jnp.bfloat16)
+            for j in range(n_fs):
+                xs[f, j, to] = two[:, j * width : (j + 1) * width]
+
+    ag_z, ag_side, ag_core, ag_fwd = {}, {}, {}, {}
+    for k in ORDER:
+        src = xs.at[f, t]
+        ag_z[k] = send(src, src, ag_s.at[0, k], ag_r.at[0, k], {"fs": (f + k) % n_fs})
+        ag_z[k].start()
+    for k in ORDER:
+        forward(k)
+
+    def spread(k):
+        ag_z[k].wait_recv()
+        src = xs.at[(f - k + n_fs) % n_fs, t]
+        ag_side[k] = send(src, src, ag_s.at[1, k], ag_r.at[1, k], side)
+        ag_side[k].start()
+        ag_core[k] = send(src, src, ag_s.at[2, k], ag_r.at[2, k], core)
+        ag_core[k].start()
+
+    def pass_on(k):
+        ag_side[k].wait_recv()
+        src = xs.at[(f - k + n_fs) % n_fs, t_side]
+        ag_fwd[k] = send(src, src, ag_s.at[3, k], ag_r.at[3, k], core)
+        ag_fwd[k].start()
+
+    rs_core, rs_side, rs_z = {}, {}, {}
+
+    def block(s):
+        z = (f - s + n_fs) % n_fs
+        small = ffn_small[f]
+
+        @pl.loop(0, n_seq)
+        def _(q):
+            at = pl.ds(pl.multiple_of(q * SEQ_LEN, SEQ_LEN), SEQ_LEN)
+            linear, gated = 0.0, 0.0
+            for j in range(n_fs):
+                act = xs[z, j, at]
+                linear = linear + dot_nt(act, ffn_all[j, 0:hid])
+                gated = gated + dot_nt(act, ffn_all[j, hid : 2 * hid])
+            linear = linear.astype(jnp.bfloat16).astype(jnp.float32)
+            gated = gated.astype(jnp.bfloat16).astype(jnp.float32)
+            act = jax.nn.gelu(conv_rows(gated, small) + small[3:4], approximate=True)
+            hidden = (act * linear).astype(jnp.bfloat16)
+            for j in range(n_fs):
+                pf[s, j % 2, j // 2, at] = dot_nn(hidden, ffn_all[j, 2 * hid : 3 * hid]).astype(jnp.bfloat16)
+
+        rs_core[s] = send(pf.at[s, 1 - c], rf.at[s], rs_s.at[0, s], rs_r.at[0, s], core)
+        rs_core[s].start()
+
+    def stage_core(s):
+        rs_core[s].wait_recv()
+        sf[s, 1 - x] = (pf[s, c, 1 - x].astype(jnp.float32) + rf[s, 1 - x].astype(jnp.float32)).astype(jnp.bfloat16)
+        rs_side[s] = send(sf.at[s, 1 - x], rxf.at[s], rs_s.at[1, s], rs_r.at[1, s], side)
+        rs_side[s].start()
+        sf[s, x] = (pf[s, c, x].astype(jnp.float32) + rf[s, x].astype(jnp.float32)).astype(jnp.bfloat16)
+
+    def stage_side(s):
+        rs_side[s].wait_recv()
+        tf[s] = (sf[s, x].astype(jnp.float32) + rxf[s].astype(jnp.float32)).astype(jnp.bfloat16)
+        if s > 0:
+            rs_z[s] = send(tf.at[s], rz.at[s], rs_s.at[2, s], rs_r.at[2, s], {"fs": (f - s + n_fs) % n_fs})
+            rs_z[s].start()
+
+    for k in ORDER:
+        ffn_y[k].wait_recv()
+    block(0)
+    spread(ORDER[0])
+    stage_core(0)
+    pass_on(ORDER[0])
+    spread(ORDER[1])
+    ag_core[ORDER[0]].wait_recv()
+    ag_fwd[ORDER[0]].wait_recv()
+    block(ORDER[0])
+    pass_on(ORDER[1])
+    spread(ORDER[2])
+    stage_core(ORDER[0])
+    ag_core[ORDER[1]].wait_recv()
+    ag_fwd[ORDER[1]].wait_recv()
+    block(ORDER[1])
+    stage_side(0)
+    pass_on(ORDER[2])
+    stage_core(ORDER[1])
+    stage_side(ORDER[0])
+    ag_core[ORDER[2]].wait_recv()
+    ag_fwd[ORDER[2]].wait_recv()
+    block(ORDER[2])
+    stage_core(ORDER[2])
+    stage_side(ORDER[1])
+    stage_side(ORDER[2])
+
+    total = tf[0].astype(jnp.float32)
+    for k in ORDER:
+        rs_z[k].wait_recv()
+        total = total + rz[k].astype(jnp.float32)
+    bf[t] = total.astype(jnp.bfloat16)
+    mine = bf.at[t]
+    fin_side = send(mine, mine, fin_s.at[0], fin_r.at[0], side)
+    fin_side.start()
+    fin_core = send(mine, mine, fin_s.at[1], fin_r.at[1], core)
+    fin_core.start()
+    fin_side.wait_recv()
+    theirs = bf.at[t_side]
+    fin_fwd = send(theirs, theirs, fin_s.at[2], fin_r.at[2], core)
+    fin_fwd.start()
+    fin_core.wait_recv()
+    fin_fwd.wait_recv()
+
+    @pl.loop(0, rows // step_rows)
+    def _(i):
+        at = pl.ds(pl.multiple_of(i * step_rows, step_rows), step_rows)
+        branch = jnp.concatenate([bf[j, at] for j in range(n_fs)], axis=1).astype(jnp.float32)
+        out[at] = (middle[at].astype(jnp.float32) + norm_rows(branch, gains[3:4])).astype(jnp.bfloat16)
+
+    groups = [mix_z, ffn_z, mix_y, ffn_y, mix_core, mix_side, mix_back]
+    groups += [ag_z, ag_side, ag_core, ag_fwd, rs_core, rs_side, rs_z]
+    for group in groups:
+        for copy in group.values():
+            copy.wait_send()
+    for copy in (fin_side, fin_core, fin_fwd):
+        copy.wait_send()
+
+
+def split_plan(
+    n_fs,
+    stream,
+    mix_pre_gain,
+    w_outer_gate,
+    w_inner_gate,
+    w_value,
+    mix_taps,
+    w_mix_out,
+    mix_post_gain,
+    ffn_pre_gain,
+    w_linear,
+    w_gated,
+    ffn_taps,
+    ffn_bias,
+    w_down,
+    ffn_post_gain,
+):
+    rows, model = stream.shape
+    width, conv_w = w_value.shape
+    units = w_linear.shape[1] // n_fs
+    hid = -(-units // PACK) * PACK
+    deep = -(-3 * hid // (2 * PACK)) * 2 * PACK
+    gains = jnp.stack([mix_pre_gain, mix_post_gain, ffn_pre_gain, ffn_post_gain])
+    mix_w = jnp.concatenate([w_outer_gate.T, w_inner_gate.T, w_value.T, w_mix_out], axis=0)
+
+    def cut(rows_of, extra):
+        pieces = rows_of.reshape(n_fs, units, width)
+        return jnp.pad(pieces, ((0, 0), (0, hid - units + extra), (0, 0)))
+
+    ffn_w = jnp.concatenate([cut(w_linear.T, 0), cut(w_gated.T, 0), cut(w_down, deep - 3 * hid)], axis=1)
+    small = jnp.concatenate([ffn_taps, ffn_bias[None]], axis=0).reshape(4, n_fs, units)
+    small = jnp.pad(small.transpose(1, 0, 2), ((0, 0), (0, 0), (0, hid - units)))
+    n_seq = rows // SEQ_LEN
+    half = jnp.bfloat16
+    vmem, dma = pltpu.VMEM, pltpu.SemaphoreType.DMA
+    return pl.pallas_call(
+        functools.partial(kernel, n_fs, conv_w, hid),
+        out_shape=jax.ShapeDtypeStruct((rows, model), half),
+        in_specs=[pl.BlockSpec(memory_space=vmem)] * 6,
+        out_specs=pl.BlockSpec(memory_space=vmem),
+        scratch_shapes=[
+            vmem((n_fs, *mix_w.shape), half),
+            vmem((n_fs, deep, width), half),
+            vmem((n_fs, n_fs, rows, width), half),
+            vmem((rows, model), half),
+            vmem((rows, model), half),
+            vmem((n_seq, 2, 2, SEQ_LEN, width), half),
+            vmem((n_seq, 2, SEQ_LEN, width), half),
+            vmem((n_seq, 2, SEQ_LEN, width), half),
+            vmem((n_seq, 2, SEQ_LEN, width), half),
+            vmem((n_seq, 2, 2, SEQ_LEN, width), half),
+            vmem((n_fs, 2, 2, rows, width), half),
+            vmem((n_fs, 2, rows, width), half),
+            vmem((n_fs, 2, rows, width), half),
+            vmem((n_fs, rows, width), half),
+            vmem((n_fs, rows, width), half),
+            vmem((n_fs, rows, width), half),
+            vmem((n_fs, rows, width), half),
+            dma((4, n_fs)),
+            dma((4, n_fs)),
+            dma((3, n_seq)),
+            dma((3, n_seq)),
+            dma((4, n_fs)),
+            dma((4, n_fs)),
+            dma((3, n_fs)),
+            dma((3, n_fs)),
+            dma((3,)),
+            dma((3,)),
+        ],
+        compiler_params=pltpu.CompilerParams(
+            collective_id=0, has_side_effects=True, vmem_limit_bytes=56 * 2**20
+        ),
+    )(stream, gains, mix_w, mix_taps, ffn_w, small)
+
+
+def on_device(rep, n_fs, n_tp, *arrays):
+    stream, w_value, w_linear = arrays[0], arrays[4], arrays[9]
+    same = n_fs == n_tp == 2 * rep == len(ORDER) + 1
+    whole = w_value.shape[0] % 128 == 0 and w_value.shape[1] % PACK == 0
+    even = w_linear.shape[1] % n_fs == 0 and stream.shape[0] % SEQ_LEN == 0
+    if same and rep == 2 and whole and even:
+        return split_plan(n_fs, *arrays)
+    return gather_plan(*arrays)
+
+
 def solution(mesh):
     in_specs = (
         P(("rep", "fs"), None),
@@ -99,6 +479,8 @@
         P(),
     )
     out_specs = P(("rep", "fs"), None)
+    sizes = mesh.shape
+    body = functools.partial(on_device, sizes["rep"], sizes["fs"], sizes["tp"])
     return jax.shard_map(
-        on_device, mesh=mesh, in_specs=in_specs, out_specs=out_specs, check_vma=False
+        body, mesh=mesh, in_specs=in_specs, out_specs=out_specs, check_vma=False
     )

time: 332 us -> 152 us (0.46)
  waiting for transfers between devices: 224 us -> 0 us
  Pallas kernels: 0 us -> 138 us
  blocking collectives: 56 us -> 0 us
  between operations: 15.2 us -> 0.04 us
  matrix products: 15.1 us -> 0 us
  other arithmetic: 16.8 us -> 5.48 us
  local copies, waits for them, and re-layouts: 2.28 us -> 7.07 us
    all_gather x3 -> x0, waiting for transfers between devices: 146 us -> none  [the longest x1 64.8 us: on_device(): full_down = lax.all_gather(w_down, 'fs', axis=1, tiled=True)]
    pallas_call x0 -> x1, Pallas kernels: none -> 138 us  [split_plan(): pl.pallas_call(functools.partial(kernel, n_fs, conv_w, hid), out_shape=ja...]
    psum x2 -> x0, waiting for transfers between devices: 76.1 us -> none  [settle(): branch = lax.psum(partial_value.astype(jnp.bfloat16), 'tp')]
    all_gather x4 -> x0, blocking collectives: 56 us -> none  [the longest x1 16 us: on_device(): lax.all_gather(w_inner_gate, 'fs', axis=0, tiled=True)]
    dot_general x5 -> x0, matrix products: 15.1 us -> none  [the longest x1 7.94 us: on_device(): partial_two = jnp.dot(hidden, full_down, preferred_element_type=jnp.float32)]
    add x2 -> x0, other arithmetic: 8.52 us -> none  [conv_three(): taps[0] * padded[:, :-2] + taps[1] * padded[:, 1:-1]]
    reduce_sum x4 -> x0, other arithmetic: 5.85 us -> none  [norm_scale(): jnp.mean(values * values, axis=-1, keepdims=True) + EPS]
    concatenate x0 -> x2, other arithmetic: none -> 4.84 us  [the longest x1 2.84 us: split_plan(): jnp.concatenate([cut(w_linear.T, 0), cut(w_gated.T, 0), cut(w_down, deep...]
  transfers between devices with their start and end apart: 5 -> 0, of which waited for: 5 -> 0; matrix products, arithmetic and copies ran while one was open for 5% -> 0% of each run, Pallas kernels for 0% -> 0%
where the time goes in v1:
time: 152 us; the launch traced here: 151 us
  Pallas kernels  138 us (91%)
  local copies, waits for them, and re-layouts  7.07 us (5%)
  other arithmetic  5.48 us (4%)
    pallas_call x1, Pallas kernels, split_plan(): pl.pallas_call(functools.partial(kernel, n_fs, conv_w, hid), out_shape=ja...  138 us

profile of v1, /device:TPU:1, one launch (start us, length us, event | category | flops | bytes accessed | tf_op | source)
XLA Modules:
  0.0 150.8 jit_solution(15514440582110516211)
XLA Ops:
  0.0 0.7 stack.15
  0.7 0.7 stack.16
  1.4 0.7 stack.17
  2.1 0.8 concatenate.17
  2.9 0.7 stack.18
  3.6 0.6 pad_maximum_fusion.1.gains
  4.2 0.8 concatenate.16
  5.1 0.6 pad.18.ffn_small
  5.7 2.0 %pad_maximum_fusion.mix_w = bf16[768,384]{1,0:T(8,128)(2,1)} fusion(bf16[192,384]{1,0:T(8,128)(2,1)} %param.21, bf16[192,384]{1,0:T(8,128)(2,1)} %bitcast.15, bf16[192,384]{1,0:T(8,128)(2,1)} %bitcast.16, bf16[192,384]{1,0:T(8,128)(2,1)} %bitcast.17), kind=kLoop, calls=%fused_computation.10 | loop fusion | flops 2359296 | bytes 1179648 | tf_op jit(solution)/shard_map/concatenate | solution.py:401
  7.7 2.8 %fusion.5.ffn_w = bf16[4,832,384]{2,1,0:T(8,128)(2,1)} fusion(bf16[4,264,384]{2,1,0:T(8,128)(2,1)} %bitcast.12, bf16[4,264,384]{2,1,0:T(8,128)(2,1)} %bitcast.13, bf16[4,264,384]{2,1,0:T(8,128)(2,1)} %bitcast.14), kind=kLoop, calls=%fused_computation.9 | loop fusion | flops 17891328 | bytes 4988928 | tf_op jit(solution)/shard_map/concatenate | solution.py:407
  10.5 138.2 %shard_map.145 = bf16[256,1536]{1,0:T(8,128)(2,1)} custom-call(bf16[256,1536]{1,0:T(8,128)(2,1)} %stream.1, f32[4,1536]{1,0:T(4,128)} %pad_maximum_fusion.1.gains, bf16[768,384]{1,0:T(8,128)(2,1)} %pad_maximum_fusion.mix_w, f32[3,192]{1,0:T(4,128)} %mix_taps.1, bf16[4,832,384]{2,1,0:T(8,128)(2,1)} %fusion.5.ffn_w, f32[4,4,272]{2,1,0:T(4,128)} %pad.18.ffn_small), custom_call_target="tpu_custom_call" | custom-call | tf_op jit(solution)/shard_map/pallas_call | solution.py:413
  148.7 2.1 %copy.18 = bf16[256,1536]{1,0:T(8,128)(2,1)} copy(bf16[256,1536]{1,0:T(8,128)(2,1)} %shard_map.145) | data formatting | bytes 1572864
  (2 shorter events, 0.0 us)

commit v2 on v1

--- a/solution.py
+++ b/solution.py
@@ -109,12 +109,23 @@
     conv_w,
     hid,
     stream,
-    gains,
-    mix_w,
+    gain_mix_pre,
+    gain_mix_post,
+    gain_ffn_pre,
+    gain_ffn_post,
+    w_outer,
+    w_inner,
+    w_value,
+    w_mix_out,
     mix_taps,
+    w_linear,
+    w_gated,
+    w_down,
+    ffn_taps,
+    ffn_bias,
+    out,
+    small_all,
     ffn_w,
-    ffn_small,
-    out,
     mix_all,
     ffn_all,
     xs,
@@ -149,9 +160,10 @@
     side = {"tp": 2 * (1 - x) + c}
     t_side = 2 * (1 - x) + c
     other = {"rep": 1 - r}
-    rows, width = stream.shape[0], mix_w.shape[1]
+    rows, width = stream.shape[0], w_value.shape[1]
+    units = w_linear.shape[1]
     n_seq = rows // SEQ_LEN
-    mix_half, ffn_half = mix_w.shape[0] // 2, ffn_w.shape[1] // 2
+    mix_half, ffn_half = mix_all.shape[1] // 2, ffn_w.shape[1] // 2
 
     def send(src, dst, ss, rs, where):
         return pltpu.make_async_remote_copy(
@@ -167,6 +179,8 @@
     peers = [core, side, other] + [{"fs": (f + k) % n_fs} for k in ORDER]
     for peer in peers:
         pl.semaphore_signal(barrier, inc=1, device_id=peer, device_id_type=pl.DeviceIdType.MESH)
+    for p, piece in enumerate((w_outer, w_inner, w_value, w_mix_out)):
+        mix_all[f, p * conv_w : (p + 1) * conv_w] = piece[...]
     pl.semaphore_wait(barrier, len(peers))
 
     mix_rows = pl.ds(pl.multiple_of(r * mix_half, PACK), mix_half)
@@ -174,8 +188,14 @@
     mix_z, ffn_z = {}, {}
     for k in ORDER:
         to = {"fs": (f + k) % n_fs}
-        mix_z[k] = send(mix_w.at[mix_rows], mix_all.at[f, mix_rows], zs_s.at[0, k], zs_r.at[0, k], to)
+        mix_z[k] = send(mix_all.at[f, mix_rows], mix_all.at[f, mix_rows], zs_s.at[0, k], zs_r.at[0, k], to)
         mix_z[k].start()
+    for p, piece in enumerate((w_linear, w_gated, w_down)):
+        end = (p + 1) * hid if p < 2 else ffn_w.shape[1]
+        edge = units // PACK * PACK
+        for j in range(n_fs):
+            ffn_w[j, p * hid + edge : end] = jnp.zeros((end - p * hid - edge, width), ffn_w.dtype)
+            ffn_w[j, p * hid : p * hid + units] = piece[j]
     for k in ORDER:
         to = {"fs": (f + k) % n_fs}
         ffn_z[k] = send(
@@ -183,8 +203,11 @@
         )
         ffn_z[k].start()
 
-    mix_all[f] = mix_w[...]
     ffn_all[f] = ffn_w[f]
+    small_all[...] = jnp.zeros(small_all.shape, jnp.float32)
+    for j in range(n_fs):
+        small_all[j, 0:3, 0:units] = ffn_taps[:, j * units : (j + 1) * units]
+        small_all[j, 3:4, 0:units] = ffn_bias[j * units : (j + 1) * units][None]
 
     def norm_rows(values, gain):
         scale = lax.rsqrt(jnp.mean(values * values, axis=-1, keepdims=True) + EPS)
@@ -195,7 +218,7 @@
     @pl.loop(0, rows // step_rows)
     def _(i):
         at = pl.ds(pl.multiple_of(i * step_rows, step_rows), step_rows)
-        normed[at] = norm_rows(stream[at].astype(jnp.float32), gains[0:1]).astype(jnp.bfloat16)
+        normed[at] = norm_rows(stream[at].astype(jnp.float32), gain_mix_pre[...][None]).astype(jnp.bfloat16)
 
     mix_y = {}
     for k in ORDER:
@@ -240,6 +263,9 @@
         bm[q, c] = (sm[q].astype(jnp.float32) + rxm[q].astype(jnp.float32)).astype(jnp.bfloat16)
         mix_back[q] = send(bm.at[q, c], bm.at[q, c], mix_s.at[2, q], mix_r.at[2, q], core)
         mix_back[q].start()
+    ag_z, ag_side, ag_core, ag_fwd = {}, {}, {}, {}
+    forward(ORDER[0])
+    forward(ORDER[1])
     for q in range(n_seq):
         mix_back[q].wait_recv()
 
@@ -248,130 +274,127 @@
             at = pl.ds(pl.multiple_of(i * step_rows, step_rows), step_rows)
             to = pl.ds(pl.multiple_of(q * SEQ_LEN + i * step_rows, step_rows), step_rows)
             branch = jnp.concatenate([bm[q, j % 2, j // 2, at] for j in range(n_fs)], axis=1)
-            mid = stream[to].astype(jnp.float32) + norm_rows(branch.astype(jnp.float32), gains[1:2])
+            mid = stream[to].astype(jnp.float32) + norm_rows(branch.astype(jnp.float32), gain_mix_post[...][None])
             mid = mid.astype(jnp.bfloat16)
             middle[to] = mid
-            two = norm_rows(mid.astype(jnp.float32), gains[2:3]).astype(jnp.bfloat16)
+            two = norm_rows(mid.astype(jnp.float32), gain_ffn_pre[...][None]).astype(jnp.bfloat16)
             for j in range(n_fs):
                 xs[f, j, to] = two[:, j * width : (j + 1) * width]
 
-    ag_z, ag_side, ag_core, ag_fwd = {}, {}, {}, {}
-    for k in ORDER:
-        src = xs.at[f, t]
-        ag_z[k] = send(src, src, ag_s.at[0, k], ag_r.at[0, k], {"fs": (f + k) % n_fs})
-        ag_z[k].start()
-    for k in ORDER:
-        forward(k)
-
-    def spread(k):
-        ag_z[k].wait_recv()
-        src = xs.at[(f - k + n_fs) % n_fs, t]
-        ag_side[k] = send(src, src, ag_s.at[1, k], ag_r.at[1, k], side)
-        ag_side[k].start()
-        ag_core[k] = send(src, src, ag_s.at[2, k], ag_r.at[2, k], core)
-        ag_core[k].start()
-
-    def pass_on(k):
-        ag_side[k].wait_recv()
-        src = xs.at[(f - k + n_fs) % n_fs, t_side]
-        ag_fwd[k] = send(src, src, ag_s.at[3, k], ag_r.at[3, k], core)
-        ag_fwd[k].start()
+        for k in ORDER:
+            src = xs.at[f, t, q * SEQ_LEN : (q + 1) * SEQ_LEN]
+            ag_z[k, q] = send(src, src, ag_s.at[0, k, q], ag_r.at[0, k, q], {"fs": (f + k) % n_fs})
+            ag_z[k, q].start()
+
+    forward(ORDER[2])
+
+    def spread(k, q):
+        ag_z[k, q].wait_recv()
+        src = xs.at[(f - k + n_fs) % n_fs, t, q * SEQ_LEN : (q + 1) * SEQ_LEN]
+        ag_side[k, q] = send(src, src, ag_s.at[1, k, q], ag_r.at[1, k, q], side)
+        ag_side[k, q].start()
+        ag_core[k, q] = send(src, src, ag_s.at[2, k, q], ag_r.at[2, k, q], core)
+        ag_core[k, q].start()
+
+    def pass_on(k, q):
+        ag_side[k, q].wait_recv()
+        src = xs.at[(f - k + n_fs) % n_fs, t_side, q * SEQ_LEN : (q + 1) * SEQ_LEN]
+        ag_fwd[k, q] = send(src, src, ag_s.at[3, k, q], ag_r.at[3, k, q], core)
+        ag_fwd[k, q].start()
 
     rs_core, rs_side, rs_z = {}, {}, {}
 
-    def block(s):
-        z = (f - s + n_fs) % n_fs
-        small = ffn_small[f]
-
-        @pl.loop(0, n_seq)
-        def _(q):
-            at = pl.ds(pl.multiple_of(q * SEQ_LEN, SEQ_LEN), SEQ_LEN)
-            linear, gated = 0.0, 0.0
-            for j in range(n_fs):
-                act = xs[z, j, at]
-                linear = linear + dot_nt(act, ffn_all[j, 0:hid])
-                gated = gated + dot_nt(act, ffn_all[j, hid : 2 * hid])
-            linear = linear.astype(jnp.bfloat16).astype(jnp.float32)
-            gated = gated.astype(jnp.bfloat16).astype(jnp.float32)
-            act = jax.nn.gelu(conv_rows(gated, small) + small[3:4], approximate=True)
-            hidden = (act * linear).astype(jnp.bfloat16)
-            for j in range(n_fs):
-                pf[s, j % 2, j // 2, at] = dot_nn(hidden, ffn_all[j, 2 * hid : 3 * hid]).astype(jnp.bfloat16)
-
-        rs_core[s] = send(pf.at[s, 1 - c], rf.at[s], rs_s.at[0, s], rs_r.at[0, s], core)
-        rs_core[s].start()
-
-    def stage_core(s):
-        rs_core[s].wait_recv()
-        sf[s, 1 - x] = (pf[s, c, 1 - x].astype(jnp.float32) + rf[s, 1 - x].astype(jnp.float32)).astype(jnp.bfloat16)
-        rs_side[s] = send(sf.at[s, 1 - x], rxf.at[s], rs_s.at[1, s], rs_r.at[1, s], side)
-        rs_side[s].start()
-        sf[s, x] = (pf[s, c, x].astype(jnp.float32) + rf[s, x].astype(jnp.float32)).astype(jnp.bfloat16)
-
-    def stage_side(s):
-        rs_side[s].wait_recv()
-        tf[s] = (sf[s, x].astype(jnp.float32) + rxf[s].astype(jnp.float32)).astype(jnp.bfloat16)
-        if s > 0:
-            rs_z[s] = send(tf.at[s], rz.at[s], rs_s.at[2, s], rs_r.at[2, s], {"fs": (f - s + n_fs) % n_fs})
-            rs_z[s].start()
+    def block(k, q):
+        if k > 0:
+            ag_core[k, q].wait_recv()
+            ag_fwd[k, q].wait_recv()
+        z = (f - k + n_fs) % n_fs
+        small = small_all[f]
+        linear, gated = 0.0, 0.0
+        for j in range(n_fs):
+            act = xs[z, j, q * SEQ_LEN : (q + 1) * SEQ_LEN]
+            linear = linear + dot_nt(act, ffn_all[j, 0:hid])
+            gated = gated + dot_nt(act, ffn_all[j, hid : 2 * hid])
+        linear = linear.astype(jnp.bfloat16).astype(jnp.float32)
+        gated = gated.astype(jnp.bfloat16).astype(jnp.float32)
+        act = jax.nn.gelu(conv_rows(gated, small) + small[3:4], approximate=True)
+        hidden = (act * linear).astype(jnp.bfloat16)
+        for j in range(n_fs):
+            pf[k, q, j % 2, j // 2] = dot_nn(hidden, ffn_all[j, 2 * hid : 3 * hid]).astype(jnp.bfloat16)
+        rs_core[k, q] = send(pf.at[k, q, 1 - c], rf.at[k, q], rs_s.at[0, k, q], rs_r.at[0, k, q], core)
+        rs_core[k, q].start()
+
+    def stage_core(k, q):
+        rs_core[k, q].wait_recv()
+        theirs = pf[k, q, c, 1 - x].astype(jnp.float32) + rf[k, q, 1 - x].astype(jnp.float32)
+        sf[k, q, 1 - x] = theirs.astype(jnp.bfloat16)
+        rs_side[k, q] = send(sf.at[k, q, 1 - x], rxf.at[k, q], rs_s.at[1, k, q], rs_r.at[1, k, q], side)
+        rs_side[k, q].start()
+        ours = pf[k, q, c, x].astype(jnp.float32) + rf[k, q, x].astype(jnp.float32)
+        sf[k, q, x] = ours.astype(jnp.bfloat16)
+
+    def stage_side(k, q):
+        rs_side[k, q].wait_recv()
+        tf[k, q] = (sf[k, q, x].astype(jnp.float32) + rxf[k, q].astype(jnp.float32)).astype(jnp.bfloat16)
+        if k > 0:
+            to = {"fs": (f - k + n_fs) % n_fs}
+            rs_z[k, q] = send(tf.at[k, q], rz.at[k, q], rs_s.at[2, k, q], rs_r.at[2, k, q], to)
+            rs_z[k, q].start()
 
     for k in ORDER:
         ffn_y[k].wait_recv()
-    block(0)
-    spread(ORDER[0])
-    stage_core(0)
-    pass_on(ORDER[0])
-    spread(ORDER[1])
-    ag_core[ORDER[0]].wait_recv()
-    ag_fwd[ORDER[0]].wait_recv()
-    block(ORDER[0])
-    pass_on(ORDER[1])
-    spread(ORDER[2])
-    stage_core(ORDER[0])
-    ag_core[ORDER[1]].wait_recv()
-    ag_fwd[ORDER[1]].wait_recv()
-    block(ORDER[1])
-    stage_side(0)
-    pass_on(ORDER[2])
-    stage_core(ORDER[1])
-    stage_side(ORDER[0])
-    ag_core[ORDER[2]].wait_recv()
-    ag_fwd[ORDER[2]].wait_recv()
-    block(ORDER[2])
-    stage_core(ORDER[2])
-    stage_side(ORDER[1])
-    stage_side(ORDER[2])
-
-    total = tf[0].astype(jnp.float32)
-    for k in ORDER:
-        rs_z[k].wait_recv()
-        total = total + rz[k].astype(jnp.float32)
-    bf[t] = total.astype(jnp.bfloat16)
-    mine = bf.at[t]
-    fin_side = send(mine, mine, fin_s.at[0], fin_r.at[0], side)
-    fin_side.start()
-    fin_core = send(mine, mine, fin_s.at[1], fin_r.at[1], core)
-    fin_core.start()
-    fin_side.wait_recv()
-    theirs = bf.at[t_side]
-    fin_fwd = send(theirs, theirs, fin_s.at[2], fin_r.at[2], core)
-    fin_fwd.start()
-    fin_core.wait_recv()
-    fin_fwd.wait_recv()
+    own = [(0, q) for q in range(n_seq)]
+    work = [(k, q) for k in ORDER for q in range(n_seq)]
+    lag = len(own)
+    every = own + work
+    for i in range(len(work) + 6):
+        if i < len(work):
+            spread(*work[i])
+        if i < lag:
+            block(*own[i])
+        if 1 <= i <= len(work):
+            pass_on(*work[i - 1])
+        if 2 <= i < len(work) + 2:
+            block(*work[i - 2])
+        if 1 <= i <= len(every):
+            stage_core(*every[i - 1])
+        if 3 <= i < len(every) + 3:
+            stage_side(*every[i - 3])
+
+    fin_side, fin_core, fin_fwd = {}, {}, {}
+    for q in range(n_seq):
+        at = slice(q * SEQ_LEN, (q + 1) * SEQ_LEN)
+        total = tf[0, q].astype(jnp.float32)
+        for k in ORDER:
+            rs_z[k, q].wait_recv()
+            total = total + rz[k, q].astype(jnp.float32)
+        bf[t, at] = total.astype(jnp.bfloat16)
+        mine = bf.at[t, at]
+        fin_side[q] = send(mine, mine, fin_s.at[0, q], fin_r.at[0, q], side)
+        fin_side[q].start()
+        fin_core[q] = send(mine, mine, fin_s.at[1, q], fin_r.at[1, q], core)
+        fin_core[q].start()
+    for q in range(n_seq):
+        fin_side[q].wait_recv()
+        theirs = bf.at[t_side, q * SEQ_LEN : (q + 1) * SEQ_LEN]
+        fin_fwd[q] = send(theirs, theirs, fin_s.at[2, q], fin_r.at[2, q], core)
+        fin_fwd[q].start()
+    for q in range(n_seq):
+        fin_core[q].wait_recv()
+        fin_fwd[q].wait_recv()
 
     @pl.loop(0, rows // step_rows)
     def _(i):
         at = pl.ds(pl.multiple_of(i * step_rows, step_rows), step_rows)
         branch = jnp.concatenate([bf[j, at] for j in range(n_fs)], axis=1).astype(jnp.float32)
-        out[at] = (middle[at].astype(jnp.float32) + norm_rows(branch, gains[3:4])).astype(jnp.bfloat16)
+        out[at] = (middle[at].astype(jnp.float32) + norm_rows(branch, gain_ffn_post[...][None])).astype(jnp.bfloat16)
 
     groups = [mix_z, ffn_z, mix_y, ffn_y, mix_core, mix_side, mix_back]
     groups += [ag_z, ag_side, ag_core, ag_fwd, rs_core, rs_side, rs_z]
+    groups += [fin_side, fin_core, fin_fwd]
     for group in groups:
         for copy in group.values():
             copy.wait_send()
-    for copy in (fin_side, fin_core, fin_fwd):
-        copy.wait_send()
 
 
 def split_plan(
@@ -397,26 +420,19 @@
     units = w_linear.shape[1] // n_fs
     hid = -(-units // PACK) * PACK
     deep = -(-3 * hid // (2 * PACK)) * 2 * PACK
-    gains = jnp.stack([mix_pre_gain, mix_post_gain, ffn_pre_gain, ffn_post_gain])
-    mix_w = jnp.concatenate([w_outer_gate.T, w_inner_gate.T, w_value.T, w_mix_out], axis=0)
-
-    def cut(rows_of, extra):
-        pieces = rows_of.reshape(n_fs, units, width)
-        return jnp.pad(pieces, ((0, 0), (0, hid - units + extra), (0, 0)))
-
-    ffn_w = jnp.concatenate([cut(w_linear.T, 0), cut(w_gated.T, 0), cut(w_down, deep - 3 * hid)], axis=1)
-    small = jnp.concatenate([ffn_taps, ffn_bias[None]], axis=0).reshape(4, n_fs, units)
-    small = jnp.pad(small.transpose(1, 0, 2), ((0, 0), (0, 0), (0, hid - units)))
+    cut = lambda rows_of: rows_of.reshape(n_fs, units, width)
     n_seq = rows // SEQ_LEN
     half = jnp.bfloat16
     vmem, dma = pltpu.VMEM, pltpu.SemaphoreType.DMA
     return pl.pallas_call(
         functools.partial(kernel, n_fs, conv_w, hid),
         out_shape=jax.ShapeDtypeStruct((rows, model), half),
-        in_specs=[pl.BlockSpec(memory_space=vmem)] * 6,
+        in_specs=[pl.BlockSpec(memory_space=vmem)] * 15,
         out_specs=pl.BlockSpec(memory_space=vmem),
         scratch_shapes=[
-            vmem((n_fs, *mix_w.shape), half),
+            vmem((n_fs, 8, hid), jnp.float32),
+            vmem((n_fs, deep, width), half),
+            vmem((n_fs, 4 * conv_w, width), half),
             vmem((n_fs, deep, width), half),
             vmem((n_fs, n_fs, rows, width), half),
             vmem((rows, model), half),
@@ -426,28 +442,44 @@
             vmem((n_seq, 2, SEQ_LEN, width), half),
             vmem((n_seq, 2, SEQ_LEN, width), half),
             vmem((n_seq, 2, 2, SEQ_LEN, width), half),
-            vmem((n_fs, 2, 2, rows, width), half),
-            vmem((n_fs, 2, rows, width), half),
-            vmem((n_fs, 2, rows, width), half),
-            vmem((n_fs, rows, width), half),
-            vmem((n_fs, rows, width), half),
-            vmem((n_fs, rows, width), half),
+            vmem((n_fs, n_seq, 2, 2, SEQ_LEN, width), half),
+            vmem((n_fs, n_seq, 2, SEQ_LEN, width), half),
+            vmem((n_fs, n_seq, 2, SEQ_LEN, width), half),
+            vmem((n_fs, n_seq, SEQ_LEN, width), half),
+            vmem((n_fs, n_seq, SEQ_LEN, width), half),
+            vmem((n_fs, n_seq, SEQ_LEN, width), half),
             vmem((n_fs, rows, width), half),
             dma((4, n_fs)),
             dma((4, n_fs)),
             dma((3, n_seq)),
             dma((3, n_seq)),
-            dma((4, n_fs)),
-            dma((4, n_fs)),
-            dma((3, n_fs)),
-            dma((3, n_fs)),
-            dma((3,)),
-            dma((3,)),
+            dma((4, n_fs, n_seq)),
+            dma((4, n_fs, n_seq)),
+            dma((3, n_fs, n_seq)),
+            dma((3, n_fs, n_seq)),
+            dma((3, n_seq)),
+            dma((3, n_seq)),
         ],
         compiler_params=pltpu.CompilerParams(
             collective_id=0, has_side_effects=True, vmem_limit_bytes=56 * 2**20
         ),
-    )(stream, gains, mix_w, mix_taps, ffn_w, small)
+    )(
+        stream,
+        mix_pre_gain,
+        mix_post_gain,
+        ffn_pre_gain,
+        ffn_post_gain,
+        w_outer_gate.T,
+        w_inner_gate.T,
+        w_value.T,
+        w_mix_out,
+        mix_taps,
+        cut(w_linear.T),
+        cut(w_gated.T),
+        cut(w_down),
+        ffn_taps,
+        ffn_bias,
+    )
 
 
 def on_device(rep, n_fs, n_tp, *arrays):

time: 152 us -> 129 us (0.85)
  Pallas kernels: 138 us -> 127 us
  other arithmetic: 5.48 us -> 0 us
  local copies, waits for them, and re-layouts: 7.07 us -> 2.06 us
    pallas_call x1, Pallas kernels: 138 us -> 127 us  [split_plan(): pl.pallas_call(functools.partial(kernel, n_fs, conv_w, hid), out_shape=ja...]
    concatenate x2 -> x0, other arithmetic: 4.84 us -> none  [the longest x1 2.84 us: split_plan(): jnp.concatenate([cut(w_linear.T, 0), cut(w_gated.T, 0), cut(w_down, deep...]
    another operation x4 -> x0, local copies, waits for them, and re-layouts: 2.81 us -> none  [split_plan(): jnp.stack([mix_pre_gain, mix_post_gain, ffn_pre_gain, ffn_post_gain])]
    concatenate x3 -> x0, local copies, waits for them, and re-layouts: 1.59 us -> none  [split_plan(): jnp.concatenate([ffn_taps, ffn_bias[None]], axis=0).reshape(4, n_fs, units)]
where the time goes in v2:
time: 129 us
  Pallas kernels  127 us (98%)
  local copies, waits for them, and re-layouts  2.06 us (2%)
    pallas_call x1, Pallas kernels, split_plan(): pl.pallas_call(functools.partial(kernel, n_fs, conv_w, hid), out_shape=ja...  127 us

profile of v2, /device:TPU:1, one launch (start us, length us, event | category | flops | bytes accessed | tf_op | source)
XLA Modules:
  0.0 129.2 jit_solution(15094823144101015535)
XLA Ops:
  0.0 127.2 %shard_map.145 = bf16[256,1536]{1,0:T(8,128)(2,1)} custom-call(bf16[256,1536]{1,0:T(8,128)(2,1)} %stream.1, f32[1536]{0:T(1024)} %gain_mix_pre.1, f32[1536]{0:T(1024)} %gain_mix_post.1, f32[1536]{0:T(1024)} %gain_ffn_pre.1, f32[1536]{0:T(1024)} %gain_ffn_post.1, bf16[192,384]{1,0:T(8,128)(2,1)} %bitcast.13, bf16[192,384]{1,0:T(8,128)(2,1)} %bitcast.14, ...), custom_call_target="tpu_custom_call" | custom-call | tf_op jit(solution)/shard_map/pallas_call | solution.py:427
  127.2 2.1 %copy.17 = bf16[256,1536]{1,0:T(8,128)(2,1)} copy(bf16[256,1536]{1,0:T(8,128)(2,1)} %shard_map.145) | data formatting | bytes 1572864

commit v3 on v2

--- a/solution.py
+++ b/solution.py
@@ -9,6 +9,7 @@
 
 SEQ_LEN = 128
 PACK = 16
+CHUNKS = 2
 
 
 EPS = 1e-06
@@ -183,25 +184,27 @@
         mix_all[f, p * conv_w : (p + 1) * conv_w] = piece[...]
     pl.semaphore_wait(barrier, len(peers))
 
-    mix_rows = pl.ds(pl.multiple_of(r * mix_half, PACK), mix_half)
-    ffn_rows = pl.ds(pl.multiple_of(r * ffn_half, PACK), ffn_half)
+    mix_cut, ffn_cut = mix_half // CHUNKS, ffn_half // CHUNKS
+    mix_rows = [pl.ds(pl.multiple_of(r * mix_half + h * mix_cut, PACK), mix_cut) for h in range(CHUNKS)]
+    ffn_rows = [pl.ds(pl.multiple_of(r * ffn_half + h * ffn_cut, PACK), ffn_cut) for h in range(CHUNKS)]
+    cuts = [(k, h) for k in ORDER for h in range(CHUNKS)]
     mix_z, ffn_z = {}, {}
-    for k in ORDER:
+    for k, h in cuts:
         to = {"fs": (f + k) % n_fs}
-        mix_z[k] = send(mix_all.at[f, mix_rows], mix_all.at[f, mix_rows], zs_s.at[0, k], zs_r.at[0, k], to)
-        mix_z[k].start()
+        src = mix_all.at[f, mix_rows[h]]
+        mix_z[k, h] = send(src, src, zs_s.at[0, k, h], zs_r.at[0, k, h], to)
+        mix_z[k, h].start()
     for p, piece in enumerate((w_linear, w_gated, w_down)):
         end = (p + 1) * hid if p < 2 else ffn_w.shape[1]
         edge = units // PACK * PACK
         for j in range(n_fs):
             ffn_w[j, p * hid + edge : end] = jnp.zeros((end - p * hid - edge, width), ffn_w.dtype)
             ffn_w[j, p * hid : p * hid + units] = piece[j]
-    for k in ORDER:
-        to = {"fs": (f + k) % n_fs}
-        ffn_z[k] = send(
-            ffn_w.at[(f + k) % n_fs, ffn_rows], ffn_all.at[f, ffn_rows], zs_s.at[1, k], zs_r.at[1, k], to
-        )
-        ffn_z[k].start()
+    for k, h in cuts:
+        to = (f + k) % n_fs
+        src, dst = ffn_w.at[to, ffn_rows[h]], ffn_all.at[f, ffn_rows[h]]
+        ffn_z[k, h] = send(src, dst, zs_s.at[1, k, h], zs_r.at[1, k, h], {"fs": to})
+        ffn_z[k, h].start()
 
     ffn_all[f] = ffn_w[f]
     small_all[...] = jnp.zeros(small_all.shape, jnp.float32)
@@ -221,13 +224,13 @@
         normed[at] = norm_rows(stream[at].astype(jnp.float32), gain_mix_pre[...][None]).astype(jnp.bfloat16)
 
     mix_y = {}
-    for k in ORDER:
-        mix_z[k].wait_recv()
-        src = mix_all.at[(f - k + n_fs) % n_fs, mix_rows]
-        mix_y[k] = send(src, src, zs_s.at[2, k], zs_r.at[2, k], other)
-        mix_y[k].start()
-    for k in ORDER:
-        mix_y[k].wait_recv()
+    for k, h in cuts:
+        mix_z[k, h].wait_recv()
+        src = mix_all.at[(f - k + n_fs) % n_fs, mix_rows[h]]
+        mix_y[k, h] = send(src, src, zs_s.at[2, k, h], zs_r.at[2, k, h], other)
+        mix_y[k, h].start()
+    for k, h in cuts:
+        mix_y[k, h].wait_recv()
 
     mix_core, mix_side, mix_back = {}, {}, {}
     for q in range(n_seq):
@@ -253,10 +256,11 @@
     ffn_y = {}
 
     def forward(k):
-        ffn_z[k].wait_recv()
-        src = ffn_all.at[(f - k + n_fs) % n_fs, ffn_rows]
-        ffn_y[k] = send(src, src, zs_s.at[3, k], zs_r.at[3, k], other)
-        ffn_y[k].start()
+        for h in range(CHUNKS):
+            ffn_z[k, h].wait_recv()
+            src = ffn_all.at[(f - k + n_fs) % n_fs, ffn_rows[h]]
+            ffn_y[k, h] = send(src, src, zs_s.at[3, k, h], zs_r.at[3, k, h], other)
+            ffn_y[k, h].start()
 
     for q in range(n_seq):
         mix_side[q].wait_recv()
@@ -341,8 +345,6 @@
             rs_z[k, q] = send(tf.at[k, q], rz.at[k, q], rs_s.at[2, k, q], rs_r.at[2, k, q], to)
             rs_z[k, q].start()
 
-    for k in ORDER:
-        ffn_y[k].wait_recv()
     own = [(0, q) for q in range(n_seq)]
     work = [(k, q) for k in ORDER for q in range(n_seq)]
     lag = len(own)
@@ -350,6 +352,9 @@
     for i in range(len(work) + 6):
         if i < len(work):
             spread(*work[i])
+        if i == 0:
+            for cut in cuts:
+                ffn_y[cut].wait_recv()
         if i < lag:
             block(*own[i])
         if 1 <= i <= len(work):
@@ -419,7 +424,7 @@
     width, conv_w = w_value.shape
     units = w_linear.shape[1] // n_fs
     hid = -(-units // PACK) * PACK
-    deep = -(-3 * hid // (2 * PACK)) * 2 * PACK
+    deep = -(-3 * hid // (2 * CHUNKS * PACK)) * 2 * CHUNKS * PACK
     cut = lambda rows_of: rows_of.reshape(n_fs, units, width)
     n_seq = rows // SEQ_LEN
     half = jnp.bfloat16
@@ -449,8 +454,8 @@
             vmem((n_fs, n_seq, SEQ_LEN, width), half),
             vmem((n_fs, n_seq, SEQ_LEN, width), half),
             vmem((n_fs, rows, width), half),
-            dma((4, n_fs)),
-            dma((4, n_fs)),
+            dma((4, n_fs, CHUNKS)),
+            dma((4, n_fs, CHUNKS)),
             dma((3, n_seq)),
             dma((3, n_seq)),
             dma((4, n_fs, n_seq)),
@@ -485,7 +490,7 @@
 def on_device(rep, n_fs, n_tp, *arrays):
     stream, w_value, w_linear = arrays[0], arrays[4], arrays[9]
     same = n_fs == n_tp == 2 * rep == len(ORDER) + 1
-    whole = w_value.shape[0] % 128 == 0 and w_value.shape[1] % PACK == 0
+    whole = w_value.shape[0] % 128 == 0 and w_value.shape[1] % (CHUNKS * PACK) == 0
     even = w_linear.shape[1] % n_fs == 0 and stream.shape[0] % SEQ_LEN == 0
     if same and rep == 2 and whole and even:
         return split_plan(n_fs, *arrays)

time: 129 us -> 127 us (0.984)
  Pallas kernels: 127 us -> 125 us
    pallas_call x1, Pallas kernels: 127 us -> 125 us  [split_plan(): pl.pallas_call(functools.partial(kernel, n_fs, conv_w, hid), out_shape=ja...]
where the time goes in v3:
time: 127 us
  Pallas kernels  125 us (98%)
  local copies, waits for them, and re-layouts  2.06 us (2%)
    pallas_call x1, Pallas kernels, split_plan(): pl.pallas_call(functools.partial(kernel, n_fs, conv_w, hid), out_shape=ja...  125 us

profile of v3, /device:TPU:1, one launch (start us, length us, event | category | flops | bytes accessed | tf_op | source)
XLA Modules:
  0.0 127.1 jit_solution(3657019522133308963)
XLA Ops:
  0.0 125.0 %shard_map.145 = bf16[256,1536]{1,0:T(8,128)(2,1)} custom-call(bf16[256,1536]{1,0:T(8,128)(2,1)} %stream.1, f32[1536]{0:T(1024)} %gain_mix_pre.1, f32[1536]{0:T(1024)} %gain_mix_post.1, f32[1536]{0:T(1024)} %gain_ffn_pre.1, f32[1536]{0:T(1024)} %gain_ffn_post.1, bf16[192,384]{1,0:T(8,128)(2,1)} %bitcast.13, bf16[192,384]{1,0:T(8,128)(2,1)} %bitcast.14, ...), custom_call_target="tpu_custom_call" | custom-call | tf_op jit(solution)/shard_map/pallas_call | solution.py:432
  125.0 2.1 %copy.17 = bf16[256,1536]{1,0:T(8,128)(2,1)} copy(bf16[256,1536]{1,0:T(8,128)(2,1)} %shard_map.145) | data formatting | bytes 1572864
